TPU v7x, 32 devices: a whole 2x2x4 slice. The times are simulated.
32 devices in a mesh: sp: 16 (over z, y, core), tp: 2 (over x).
Axes of the slice: x: 2, y: 2, z: 4, core: 2. Of those that a mesh axis runs over, the one named last changes fastest.
Arguments:
- target: bfloat16 [2048, 2048], P('sp'), may hold values from -0.375 to 0.375
- source: bfloat16 [4096, 2048], P(('sp', 'tp')), may hold values from -0.375 to 0.375
- target_gain: float32 [2048], replicated, may hold values from 0.3 to 12
- source_gain: float32 [2048], replicated, may hold values from 0.3 to 12
- w_query: bfloat16 [2048, 1024], P(None, 'tp'), may hold values from -0.125 to 0.125
- w_key: bfloat16 [2048, 256], replicated, may hold values from -0.125 to 0.125
- w_value: bfloat16 [2048, 256], replicated, may hold values from -0.125 to 0.125
- attended: bfloat16 [2048, 1024], P('sp', 'tp'), may hold values from -6 to 6
- d_attended: bfloat16 [2048, 1024], P('sp', 'tp'), may hold values from -24 to 24
Outputs:
- d_target: bfloat16 [2048, 2048], P('sp')
- d_source: float32 [4096, 2048], P(('sp', 'tp'))
- d_w_query: float32 [2048, 1024], P('sp', 'tp')
All inputs are finite; a program needn't handle non-finite values.
Results may differ from a plain program's by a relative error of at most 0.02.
The roundings to bfloat16 on the way count: a program that leaves them out, or rounds other values in their place, can miss the bound.
Values may be sent and summed in bfloat16 or wider, within the bound.
A program may use at most 64 MiB of HBM per device.

v0:
```python
import jax
import jax.numpy as jnp
from jax import lax
from jax.sharding import PartitionSpec as P

KVH = 2
HD = 128
EPS = 1e-06


def merged(shard, axis, combine):
    everything = jax.tree.map(lambda part: lax.all_gather(part, axis), shard)
    leading = jax.tree.map(lambda part: part[0], everything)

    def turn(k, so_far):
        return combine(so_far, jax.tree.map(lambda part: part[k], everything))

    return lax.fori_loop(1, lax.axis_size(axis), turn, leading)


def norm_rows(matrix, gain_vector):
    widened = matrix.astype(jnp.float32)
    inverse = lax.rsqrt(jnp.mean(widened * widened, axis=-1, keepdims=True) + EPS)
    return widened * inverse * gain_vector


def norm_back(matrix, gain_vector, cotangent):
    _, pullback = jax.vjp(lambda values: norm_rows(values, gain_vector), matrix.astype(jnp.float32))
    return pullback(cotangent)[0]


def block_count(row_count, most_rows):
    number = 1
    while row_count % (number * 2) == 0 and row_count // number > most_rows:
        number = number * 2
    return number


def merge_totals(earlier, latter):
    maxima = jnp.maximum(earlier[0], latter[0])
    totals = earlier[1] * jnp.exp(earlier[0] - maxima) + latter[1] * jnp.exp(latter[0] - maxima)
    return (maxima, totals)


def block_totals(queries, key_head, scaling):
    row_count = queries.shape[0]
    per_head = queries.reshape(row_count, -1, key_head.shape[1])
    scores = (
        jnp.einsum("rhd,sd->rhs", per_head, key_head, preferred_element_type=jnp.float32) * scaling
    )
    maxima = jnp.max(scores, axis=-1)
    totals = jnp.sum(jnp.exp(scores - maxima[..., None]), axis=-1)
    return (maxima, totals)


def score_grads(query_heads, grad_heads, delta_rows, log_total, key_head, value_head, scaling):
    scores = (
        jnp.einsum("rhd,sd->rhs", query_heads, key_head, preferred_element_type=jnp.float32)
        * scaling
    )
    weights = jnp.exp(scores - log_total[..., None])
    d_weights = jnp.einsum(
        "rhd,sd->rhs", grad_heads, value_head, preferred_element_type=jnp.float32
    )
    d_scores = (weights * (d_weights - delta_rows.astype(jnp.float32)[..., None])).astype(
        jnp.bfloat16
    )
    return (weights, d_scores)


def gradient_block(carried, blocks, key_head, value_head, scaling):
    key_acc, value_acc = carried
    queries, cotangent, delta_rows, log_total = blocks
    row_count = queries.shape[0]
    head_dim = key_head.shape[1]
    query_heads = queries.reshape(row_count, -1, head_dim)
    grad_heads = cotangent.reshape(row_count, -1, head_dim)
    weights, d_scores = score_grads(
        query_heads, grad_heads, delta_rows, log_total, key_head, value_head, scaling
    )
    key_acc = (
        key_acc
        + jnp.einsum("rhs,rhd->sd", d_scores, query_heads, preferred_element_type=jnp.float32)
        * scaling
    )
    value_acc = value_acc + jnp.einsum(
        "rhs,rhd->sd", weights.astype(jnp.bfloat16), grad_heads, preferred_element_type=jnp.float32
    )
    return ((key_acc, value_acc), None)


def local(target, source, target_gain, source_gain, w_query, w_key, w_value, attended, d_attended):
    tp_size = lax.axis_size("tp")
    local_rows = target.shape[0]
    source_rows = source.shape[0]
    query_width = w_query.shape[1]
    scaling = HD ** (-0.5)
    normed_target = norm_rows(target, target_gain).astype(jnp.bfloat16)
    normed_source = norm_rows(source, source_gain).astype(jnp.bfloat16)
    query = jnp.dot(normed_target, w_query, preferred_element_type=jnp.float32).astype(jnp.bfloat16)
    key_own = jnp.dot(normed_source, w_key, preferred_element_type=jnp.float32).astype(jnp.bfloat16)
    value_own = jnp.dot(normed_source, w_value, preferred_element_type=jnp.float32).astype(
        jnp.bfloat16
    )
    key_block, value_block = (
        lax.all_gather(key_own, "tp", axis=0, tiled=True),
        lax.all_gather(value_own, "tp", axis=0, tiled=True),
    )
    group_size = tp_size // KVH
    kv_index = lax.axis_index("tp") // group_size
    key_head = lax.dynamic_slice_in_dim(key_block, kv_index * HD, HD, 1)
    value_head = lax.dynamic_slice_in_dim(value_block, kv_index * HD, HD, 1)
    delta = jnp.einsum(
        "rhd,rhd->rh",
        d_attended.reshape(local_rows, -1, HD),
        attended.reshape(local_rows, -1, HD),
        preferred_element_type=jnp.float32,
    ).astype(jnp.bfloat16)
    all_queries = lax.all_gather(query, "sp", axis=0, tiled=True)
    target_total = all_queries.shape[0]
    number = block_count(target_total, 512)
    maxima, totals = lax.map(
        lambda blocked: block_totals(blocked, key_head, scaling),
        all_queries.reshape(number, target_total // number, query_width),
    )
    maxima = maxima.reshape(target_total, -1)
    totals = totals.reshape(target_total, -1)
    maxima, totals = merged((maxima, totals), "sp", merge_totals)
    log_total = maxima + jnp.log(totals)
    block_rows = key_head.shape[0]
    start_state = (
        jnp.zeros((block_rows, HD), jnp.float32),
        jnp.zeros((block_rows, HD), jnp.float32),
    )
    key_acc = start_state[0]
    value_acc = start_state[1]
    cotangent = lax.all_gather(d_attended, "sp", axis=0, tiled=True)
    delta_piece = lax.all_gather(delta, "sp", axis=0, tiled=True)
    row_count = cotangent.shape[0]
    pieces_count = block_count(row_count, 512)
    blocked = tuple(
        (
            member.reshape((pieces_count, row_count // pieces_count) + member.shape[1:])
            for member in (all_queries, cotangent, delta_piece, log_total)
        )
    )

    def fold_inner_step(state, blocks):
        return gradient_block(state, blocks, key_head, value_head, scaling)

    (key_acc, value_acc), grad_rows = lax.scan(fold_inner_step, (key_acc, value_acc), blocked)
    folded = (key_acc, value_acc)
    key_acc = folded[0]
    value_acc = folded[1]
    own_totals = lax.dynamic_slice_in_dim(
        log_total, lax.axis_index("sp") * local_rows, local_rows, 0
    )
    own_queries = query.reshape(local_rows, -1, HD)
    own_grads = d_attended.reshape(local_rows, -1, HD)
    query_start = jnp.zeros((local_rows, query_width // HD, HD), jnp.float32)
    keys_piece = lax.all_gather(key_head, "sp", axis=0, tiled=True)
    values_piece = lax.all_gather(value_head, "sp", axis=0, tiled=True)
    row_count = keys_piece.shape[0]
    pieces_count = block_count(row_count, 512)
    key_blocks = keys_piece.reshape(pieces_count, row_count // pieces_count, HD)
    value_blocks = values_piece.reshape(pieces_count, row_count // pieces_count, HD)

    def key_inner_step(state, blocks):
        keys_now, values_now = blocks
        _, d_scores = score_grads(
            own_queries, own_grads, delta, own_totals, keys_now, values_now, scaling
        )
        return (
            state
            + jnp.einsum("rhs,sd->rhd", d_scores, keys_now, preferred_element_type=jnp.float32)
            * scaling,
            None,
        )

    result, _ = lax.scan(key_inner_step, query_start, (key_blocks, value_blocks))
    d_query = result.reshape(local_rows, query_width).astype(jnp.bfloat16)
    d_w_query = lax.psum_scatter(
        jnp.einsum("rd,rc->dc", normed_target, d_query, preferred_element_type=jnp.float32),
        "sp",
        scatter_dimension=0,
        tiled=True,
    )
    partial_value = jnp.einsum("rc,dc->rd", d_query, w_query, preferred_element_type=jnp.float32)
    d_normed = lax.psum(partial_value.astype(jnp.bfloat16), "tp").astype(jnp.float32)
    d_target = norm_back(target, target_gain, d_normed).astype(jnp.bfloat16)
    stacked = jnp.stack([key_acc, value_acc], axis=1).reshape(tp_size, source_rows, 2 * HD)
    returned = lax.all_to_all(
        stacked.astype(jnp.bfloat16), "tp", split_axis=0, concat_axis=0, tiled=True
    ).astype(stacked.dtype)
    grouped = returned.reshape(KVH, group_size, source_rows, 2, HD).sum(axis=1)
    d_key = (
        grouped[:, :, 0, :].transpose(1, 0, 2).reshape(source_rows, KVH * HD).astype(jnp.bfloat16)
    )
    d_value = (
        grouped[:, :, 1, :].transpose(1, 0, 2).reshape(source_rows, KVH * HD).astype(jnp.bfloat16)
    )
    d_normed_source = jnp.einsum(
        "rc,dc->rd", d_key, w_key, preferred_element_type=jnp.float32
    ) + jnp.einsum("rc,dc->rd", d_value, w_value, preferred_element_type=jnp.float32)
    d_source = norm_back(source, source_gain, d_normed_source)
    return (d_target, d_source, d_w_query)


def solution(mesh):
    return jax.shard_map(
        local,
        mesh=mesh,
        in_specs=(
            P("sp", None),
            P(("sp", "tp"), None),
            P(),
            P(),
            P(None, "tp"),
            P(),
            P(),
            P("sp", "tp"),
            P("sp", "tp"),
        ),
        out_specs=(P("sp", None), P(("sp", "tp"), None), P("sp", "tp")),
        check_vma=False,
    )
```

profile of v0, /device:TPU:0, one launch (start us, length us, event | category | flops | bytes accessed | tf_op | source)
XLA Modules:
  0.0 290.3 jit_solution(17529582570570535842)
XLA Ops:
  8.9 2.2 convolution_convert_fusion.1
  13.6 6.0 %all_gather.27 = bf16[256,256]{1,0:T(8,128)(2,1)S(1)} all-gather(bf16[128,256]{1,0:T(8,128)(2,1)S(1)} %convolution_convert_fusion.3), channel_id=1, replica_groups=mesh['sp'=16,'tp'=2] {'tp'}, dimensions={0}, use_global_device_ids=true | all-gather | bytes 196608 | tf_op jit(solution)/shard_map/all_gather | solution.py:106
  21.9 4.9 %all_gather.32 = bf16[256,256]{1,0:T(8,128)(2,1)S(1)} all-gather(bf16[128,256]{1,0:T(8,128)(2,1)S(1)} %convolution_convert_fusion.2), channel_id=1, replica_groups=mesh['sp'=16,'tp'=2] {'tp'}, dimensions={0}, use_global_device_ids=true | all-gather | bytes 196608 | tf_op jit(solution)/shard_map/all_gather | solution.py:107
  30.3 25.2 %all-gather.7.cloned.1.call-done = bf16[2048,512]{1,0:T(8,128)(2,1)} async-done(((bf16[128,512]{1,0:T(8,128)(2,1)}), bf16[2048,512]{1,0:T(8,128)(2,1)}) %all-gather.7.cloned.1.call-update) | async-done | bytes 2097168 | tf_op jit(solution)/shard_map/all_gather | solution.py:119
  55.5 4.2 %copy.78 = bf16[4,512,512]{1,2,0:T(8,128)(2,1)} copy(bf16[4,512,512]{2,1,0:T(8,128)(2,1)} %bitcast.167) | data formatting | bytes 4194304 | tf_op jit(solution)/shard_map/while | solution.py:122
  59.7 7.7 %while.53 = (s32[]{:T(128)}, f32[4,512,4]{1,2,0:T(4,128)S(1)}, f32[4,512,4]{1,2,0:T(4,128)S(1)}, bf16[4,512,512]{1,2,0:T(8,128)(2,1)}, bf16[256,128]{1,0:T(8,128)(2,1)S(1)}, /*index=5*/s32[]{:T(128)}) while((s32[]{:T(128)}, f32[4,512,4]{1,2,0:T(4,128)S(1)}, f32[4,512,4]{1,2,0:T(4,128)S(1)}, bf16[4,512,512]{1,2,0:T(8,128)(2,1)}, ...), condition=%wide.region_5.6_spmd, body=%wide.region_2.5_spmd.sunk | while | flops 136835072 | bytes 5890125 | solution.py:122
  67.4 20.9 %all_gather.31 = f32[16,2048,4]{1,2,0:T(4,128)S(1)} all-gather(f32[1,2048,4]{1,2,0:T(4,128)S(1)} %bitcast.179), channel_id=1, replica_groups=mesh['sp'=16,'tp'=2] {'sp'}, dimensions={0}, use_global_device_ids=true | all-gather | bytes 557056 | tf_op jit(solution)/shard_map/all_gather | solution.py:12
  88.3 19.2 %all_gather.30 = f32[16,2048,4]{1,2,0:T(4,128)S(1)} all-gather(f32[1,2048,4]{1,2,0:T(4,128)} %bitcast.178), channel_id=1, replica_groups=mesh['sp'=16,'tp'=2] {'sp'}, dimensions={0}, use_global_device_ids=true | all-gather | bytes 557056 | tf_op jit(solution)/shard_map/all_gather | solution.py:12
  108.7 25.1 %all-gather.9.cloned.1.call-done = bf16[4096,128]{1,0:T(8,128)(2,1)} async-done(((bf16[256,128]{1,0:T(8,128)(2,1)}), bf16[4096,128]{1,0:T(8,128)(2,1)}) %all-gather.9.cloned.1.call-update) | async-done | bytes 1048592 | tf_op jit(solution)/shard_map/all_gather | solution.py:162
  133.7 24.7 %while.55 = (s32[]{:T(128)}, f32[128,4,128]{2,0,1:T(8,128)S(1)}, bf16[8,512,128]{2,1,0:T(8,128)(2,1)}, bf16[128,4,128]{2,0,1:T(8,128)(2,1)}, f32[128,4]{0,1:T(4,...) while((s32[]{:T(128)}, f32[128,4,128]{2,0,1:T(8,128)S(1)}, ...), condition=%wide.region_9.10_spmd.clone, body=%wide.region_8.9_spmd.clone.sunk | while | flops 202834432 | bytes 3285615 | solution.py:180
  160.3 19.4 %all_gather.35 = bf16[2048,4]{0,1:T(4,128)(2,1)S(1)} all-gather(bf16[128,4]{0,1:T(4,128)(2,1)S(1)} %get-tuple-element.772), channel_id=1, replica_groups=mesh['sp'=16,'tp'=2] {'sp'}, dimensions={0}, use_global_device_ids=true | all-gather | bytes 17408 | tf_op jit(solution)/shard_map/all_gather | solution.py:138
  179.7 2.7 fusion.52
  183.3 42.9 %while.56 = (s32[]{:T(128)}, f32[256,128]{1,0:T(8,128)}, f32[256,128]{1,0:T(8,128)S(1)}, bf16[4,512,512]{1,2,0:T(8,128)(2,1)}, bf16[256,128]{1,0:T(8,128)(2,1)S(...) while((s32[]{:T(128)}, f32[256,128]{1,0:T(8,128)}, ...), condition=%wide.region_13.14_spmd.clone, body=%wide.region_12.13_spmd.clone.sunk | while | flops 541231104 | bytes 14340260 | solution.py:151
  187.6 3.8 %fusion.113 = f32[256,128]{1,0:T(8,128)} fusion(bf16[512,4,128]{0,2,1:T(8,128)(2,1)} %bitcast.164, f32[512,4,256]{2,0,1:T(8,128)} %fusion.112, bf16[512,4,128]{0,2,1:T(8,128)(2,1)S(1)} %bitcast.161, f32[512,4]{0,1:T(4,128)S(1)} %bitcast_convert_fusion.2, f32[512,4]{0,1:T(4,128)S(1)} %dynamic-slice_bitcast_fusion.2, ...), kind=kOutput, calls=%fused_computation.39.clone.1 | convolution fusion | flops 271155200 | bytes 3489793 | tf_op jit(solution)/shard_map/while/body/eval_jaxpr/rhs,rhd->sd/dot_general | solution.py:83
  191.5 2.4 fusion.114
  198.3 3.9 %fusion.113 = f32[256,128]{1,0:T(8,128)} fusion(bf16[512,4,128]{0,2,1:T(8,128)(2,1)} %bitcast.164, f32[512,4,256]{2,0,1:T(8,128)} %fusion.112, bf16[512,4,128]{0,2,1:T(8,128)(2,1)S(1)} %bitcast.161, f32[512,4]{0,1:T(4,128)S(1)} %bitcast_convert_fusion.2, f32[512,4]{0,1:T(4,128)S(1)} %dynamic-slice_bitcast_fusion.2, ...), kind=kOutput, calls=%fused_computation.39.clone.1 | convolution fusion | flops 271155200 | bytes 3489793 | tf_op jit(solution)/shard_map/while/body/eval_jaxpr/rhs,rhd->sd/dot_general | solution.py:83
  202.2 2.4 fusion.114
  208.9 3.9 %fusion.113 = f32[256,128]{1,0:T(8,128)} fusion(bf16[512,4,128]{0,2,1:T(8,128)(2,1)} %bitcast.164, f32[512,4,256]{2,0,1:T(8,128)} %fusion.112, bf16[512,4,128]{0,2,1:T(8,128)(2,1)S(1)} %bitcast.161, f32[512,4]{0,1:T(4,128)S(1)} %bitcast_convert_fusion.2, f32[512,4]{0,1:T(4,128)S(1)} %dynamic-slice_bitcast_fusion.2, ...), kind=kOutput, calls=%fused_computation.39.clone.1 | convolution fusion | flops 271155200 | bytes 3489793 | tf_op jit(solution)/shard_map/while/body/eval_jaxpr/rhs,rhd->sd/dot_general | solution.py:83
  212.8 2.4 fusion.114
  219.7 4.0 %fusion.113 = f32[256,128]{1,0:T(8,128)} fusion(bf16[512,4,128]{0,2,1:T(8,128)(2,1)} %bitcast.164, f32[512,4,256]{2,0,1:T(8,128)} %fusion.112, bf16[512,4,128]{0,2,1:T(8,128)(2,1)S(1)} %bitcast.161, f32[512,4]{0,1:T(4,128)S(1)} %bitcast_convert_fusion.2, f32[512,4]{0,1:T(4,128)S(1)} %dynamic-slice_bitcast_fusion.2, ...), kind=kOutput, calls=%fused_computation.39.clone.1 | convolution fusion | flops 271155200 | bytes 3489793 | tf_op jit(solution)/shard_map/while/body/eval_jaxpr/rhs,rhd->sd/dot_general | solution.py:83
  223.7 2.5 fusion.114
  227.5 6.9 %all_to_all.5 = bf16[2,128,256]{2,1,0:T(8,128)(2,1)S(1)} all-to-all(bf16[2,128,256]{2,1,0:T(8,128)(2,1)S(1)} %convert_element_type.103), channel_id=1, replica_groups=mesh['sp'=16,'tp'=2] {'tp'}, dimensions={0} | all-to-all | bytes 262144 | tf_op jit(solution)/shard_map/all_to_all | solution.py:192
  239.9 2.2 fusion.43
  242.1 41.4 %reduce-scatter.2.cloned.1.call-done = f32[128,512]{1,0:T(8,128)} async-done(((f32[2048,512]{1,0:T(8,128)}), f32[128,512]{1,0:T(8,128)}) %reduce-scatter.2.cloned.1.call-update) | async-done | bytes 262160 | tf_op jit(solution)/shard_map/reduce_scatter | solution.py:182
  (183 shorter events, 70.1 us)
Async XLA Ops:
  7.2 4.0 %copy-start.5 = (bf16[128,2048]{1,0:T(8,128)(2,1)S(1)}, bf16[128,2048]{1,0:T(8,128)(2,1)}, u32[]{:S(2)}) copy-start(bf16[128,2048]{1,0:T(8,128)(2,1)} %param.18) | copy-start | bytes 1572868
  7.2 4.8 %copy-start.14 = (f32[2048]{0:T(1024)S(1)}, f32[2048]{0:T(1024)}, u32[]{:S(2)}) copy-start(f32[2048]{0:T(1024)} %param.20) | copy-start | bytes 24580
  7.2 48.3 %all-gather.7.cloned.1.call-start = ((), (), s32[]{:S(2)}) async-start(), calls=%async_computation.3 | async-start | bytes 2228224 | tf_op jit(solution)/shard_map/all_gather | solution.py:119
  8.6 2.8 copy-start.15
  11.1 97.5 %all-gather.5.cloned.1.call-start = ((), (), s32[]{:S(2)}) async-start(), calls=%async_computation.2 | async-start | bytes 1114112 | tf_op jit(solution)/shard_map/all_gather | solution.py:161
  11.9 14.9 %copy-start.17 = (f32[128]{0:T(128)}, f32[128]{0:T(128)S(1)}, u32[]{:S(2)}) copy-start(f32[128]{0:T(128)S(1)} %fusion.57) | copy-start | bytes 1540
  11.9 16.2 %copy-start.8 = (bf16[128,512]{1,0:T(8,128)(2,1)S(1)}, bf16[128,512]{1,0:T(8,128)(2,1)}, u32[]{:S(2)}) copy-start(bf16[128,512]{1,0:T(8,128)(2,1)} %param.25) | copy-start | bytes 393220
  12.0 16.3 %copy-start.9 = (bf16[128,512]{1,0:T(8,128)(2,1)S(1)}, bf16[128,512]{1,0:T(8,128)(2,1)}, u32[]{:S(2)}) copy-start(bf16[128,512]{1,0:T(8,128)(2,1)} %convolution_convert_fusion.1) | copy-start | bytes 393220
  13.6 16.3 %copy-start.11 = (bf16[128,512]{1,0:T(8,128)(2,1)S(1)}, bf16[128,512]{1,0:T(8,128)(2,1)}, u32[]{:S(2)}) copy-start(bf16[128,512]{1,0:T(8,128)(2,1)} %param.24) | copy-start | bytes 393220
  20.3 113.5 %all-gather.9.cloned.1.call-start = ((), (), s32[]{:S(2)}) async-start(), calls=%async_computation.4 | async-start | bytes 1114112 | tf_op jit(solution)/shard_map/all_gather | solution.py:162
  27.5 155.0 %all-gather.11.cloned.1.call-start = ((), (), s32[]{:S(2)}) async-start(), calls=%async_computation.6 | async-start | bytes 2228224 | tf_op jit(solution)/shard_map/all_gather | solution.py:137
  28.1 210.5 %all-reduce.2.cloned.1.call-start = ((), (), s32[]{:S(2)}) async-start(), calls=%async_computation.5 | async-start | bytes 1048576 | tf_op jit(solution)/shard_map/psum | solution.py:189
  55.5 4.2 %copy-start.2 = (bf16[256,128]{1,0:T(8,128)(2,1)S(1)}, bf16[256,128]{1,0:T(8,128)(2,1)}, u32[]{:S(2)}) copy-start(bf16[256,128]{1,0:T(8,128)(2,1)} %constant_dynamic-slice_fusion.5) | copy-start | bytes 196612
  67.4 20.9 %copy-start.13 = (f32[4,512,4]{1,2,0:T(4,128)}, f32[4,512,4]{1,2,0:T(4,128)S(1)}, u32[]{:S(2)}) copy-start(f32[4,512,4]{1,2,0:T(4,128)S(1)} %get-tuple-element.254) | copy-start | bytes 98308
  158.4 21.3 %copy-start.3 = (bf16[128,2048]{1,0:T(8,128)(2,1)S(1)}, bf16[128,2048]{1,0:T(8,128)(2,1)}, u32[]{:S(2)}) copy-start(bf16[128,2048]{1,0:T(8,128)(2,1)} %param.17) | copy-start | bytes 1572868
  158.4 21.3 %copy-start.12 = (f32[2048]{0:T(1024)S(1)}, f32[2048]{0:T(1024)}, u32[]{:S(2)}) copy-start(f32[2048]{0:T(1024)} %param.19) | copy-start | bytes 24580
  160.2 123.3 %reduce-scatter.2.cloned.1.call-start = ((), (), s32[]{:S(2)}) async-start(), calls=%async_computation.7 | async-start | bytes 4456448 | tf_op jit(solution)/shard_map/reduce_scatter | solution.py:182
  184.4 1.9 copy-start.1
  195.0 1.9 copy-start.1
  205.7 1.9 copy-start.1
  216.4 1.9 copy-start.1
  227.2 9.5 %copy-start.6 = (bf16[128,2048]{1,0:T(8,128)(2,1)S(1)}, bf16[128,2048]{1,0:T(8,128)(2,1)}, u32[]{:S(2)}) copy-start(bf16[128,2048]{1,0:T(8,128)(2,1)} %param.18) | copy-start | bytes 1572868
  234.9 1.8 copy-start.7
  237.3 2.6 copy-start.16
  (6 other events, 5.7 us)
Sparse Core Ops, SparseCore 0:
  11.3 44.1 all-gather.6
  57.6 36.9 all-gather.4
  96.8 36.9 all-gather.8
  135.7 40.4 all-gather.10
  178.9 27.3 all-reduce.1
  210.6 72.8 reduce-scatter.1
where the time goes:
time: 292 us; the launch traced here: 290 us
  waiting for transfers between devices  92.4 us (32%)
  blocking collectives  77.4 us (27%)
  matrix products  71.2 us (24%)
  local copies, waits for them, and re-layouts  23.9 us (8%)
  between operations  14.5 us (5%)
  other arithmetic  9.92 us (3%)
    reduce_scatter x1, waiting for transfers between devices, local(): lax.psum_scatter(jnp.einsum('rd,rc->dc', normed_target, d_query, preferre...  41.4 us
    all_gather x2, blocking collectives, merged(): everything = jax.tree.map(lambda part: lax.all_gather(part, axis), shard)  40.1 us
    all_gather x1, waiting for transfers between devices, local(): all_queries = lax.all_gather(query, 'sp', axis=0, tiled=True)  25.2 us
    all_gather x1, waiting for transfers between devices, local(): values_piece = lax.all_gather(value_head, 'sp', axis=0, tiled=True)  25.1 us
    all_gather x1, blocking collectives, local(): delta_piece = lax.all_gather(delta, 'sp', axis=0, tiled=True)  19.4 us
    dot_general x4, matrix products, gradient_block(): jnp.einsum('rhs,rhd->sd', d_scores, query_heads, preferred_element_type=j...  15.7 us
    dot_general x8, matrix products, key_inner_step(): jnp.einsum('rhs,sd->rhd', d_scores, keys_now, preferred_element_type=jnp....  14.2 us
    dynamic_slice x16, local copies, waits for them, and re-layouts, local(): lax.map(lambda blocked: block_totals(blocked, key_head, scaling), all_que...  13.9 us
  transfers between devices with their start and end apart: 6, of which 3 were waited for; matrix products, arithmetic and copies ran while one was open for 34% of the time, Pallas kernels for 0%

commit v1 on v0

--- a/solution.py
+++ b/solution.py
@@ -6,6 +6,20 @@
 KVH = 2
 HD = 128
 EPS = 1e-06
+
+
+def _pair_clusters(sheet, device_axis):
+    buffers = []
+    n_dev_all = lax.axis_size(device_axis)
+    for i in range(n_dev_all):
+        buffers.append((i, (i + 1) % n_dev_all))
+    f_now = [None] * n_dev_all
+    f_now[n_dev_all - 1] = sheet
+    for m in range(n_dev_all - 2, -1, -1):
+        f_now[m] = lax.ppermute(f_now[m + 1], device_axis, buffers)
+    v_now = jnp.concatenate(f_now, axis=0)
+    y2 = lax.axis_index(device_axis)
+    return jnp.roll(v_now, (y2 + 1) * sheet.shape[0], axis=0)
 
 
 def merged(shard, axis, combine):
@@ -159,7 +173,7 @@
     own_grads = d_attended.reshape(local_rows, -1, HD)
     query_start = jnp.zeros((local_rows, query_width // HD, HD), jnp.float32)
     keys_piece = lax.all_gather(key_head, "sp", axis=0, tiled=True)
-    values_piece = lax.all_gather(value_head, "sp", axis=0, tiled=True)
+    values_piece = _pair_clusters(value_head, device_axis="sp")
     row_count = keys_piece.shape[0]
     pieces_count = block_count(row_count, 512)
     key_blocks = keys_piece.reshape(pieces_count, row_count // pieces_count, HD)

time: 292 us -> 326 us (1.12)
  waiting for transfers between devices: 92.4 us -> 124 us
  local copies, waits for them, and re-layouts: 23.9 us -> 31.2 us
    ppermute x0 -> x15, waiting for transfers between devices: none -> 96.6 us  [_pair_clusters(): f_now[m] = lax.ppermute(f_now[m + 1], device_axis, buffers)]
    all_gather x1, waiting for transfers between devices: 25.2 us -> 0.01 us  [local(): all_queries = lax.all_gather(query, 'sp', axis=0, tiled=True)]
    all_gather x1 -> x0, waiting for transfers between devices: 25.1 us -> none  [local(): values_piece = lax.all_gather(value_head, 'sp', axis=0, tiled=True)]
    reduce_scatter x1, waiting for transfers between devices: 41.4 us -> 27.2 us  [local(): lax.psum_scatter(jnp.einsum('rd,rc->dc', normed_target, d_query, preferre...]
    unnamed x44 -> x79, local copies, waits for them, and re-layouts: 3.42 us -> 8.67 us
  transfers between devices with their start and end apart: 6 -> 20, of which waited for: 3 -> 16; matrix products, arithmetic and copies ran while one was open for 34% -> 32% of each run, Pallas kernels for 0% -> 0%
where the time goes in v1:
time: 326 us; the launch traced here: 324 us
  waiting for transfers between devices  124 us (38%)
  blocking collectives  75.1 us (23%)
  matrix products  68.9 us (21%)
  local copies, waits for them, and re-layouts  31.2 us (10%)
  between operations  14.3 us (4%)
  other arithmetic  9.59 us (3%)
    ppermute x15, waiting for transfers between devices, _pair_clusters(): f_now[m] = lax.ppermute(f_now[m + 1], device_axis, buffers)  96.6 us
    all_gather x2, blocking collectives, merged(): everything = jax.tree.map(lambda part: lax.all_gather(part, axis), shard)  39.6 us
    reduce_scatter x1, waiting for transfers between devices, local(): lax.psum_scatter(jnp.einsum('rd,rc->dc', normed_target, d_query, preferre...  27.2 us
    all_gather x1, blocking collectives, local(): delta_piece = lax.all_gather(delta, 'sp', axis=0, tiled=True)  17.5 us
    dot_general x8, matrix products, key_inner_step(): jnp.einsum('rhs,sd->rhd', d_scores, keys_now, preferred_element_type=jnp....  14.2 us
    dynamic_slice x16, local copies, waits for them, and re-layouts, local(): lax.map(lambda blocked: block_totals(blocked, key_head, scaling), all_que...  13.9 us
    dot_general x4, matrix products, gradient_block(): jnp.einsum('rhs,rhd->sd', d_scores, query_heads, preferred_element_type=j...  13.2 us
    dot_general x8, matrix products, score_grads(): jnp.einsum('rhd,sd->rhs', grad_heads, value_head, preferred_element_type=...  10.1 us
  transfers between devices with their start and end apart: 20, of which 16 were waited for; matrix products, arithmetic and copies ran while one was open for 32% of the time, Pallas kernels for 0%

profile of v1, /device:TPU:0, one launch (start us, length us, event | category | flops | bytes accessed | tf_op | source)
XLA Modules:
  0.0 324.2 jit_solution(10792523218728184396)
XLA Ops:
  13.6 5.9 %all_gather.24 = bf16[256,256]{1,0:T(8,128)(2,1)S(1)} all-gather(bf16[128,256]{1,0:T(8,128)(2,1)S(1)} %convolution_convert_fusion.3), channel_id=1, replica_groups=mesh['sp'=16,'tp'=2] {'tp'}, dimensions={0}, use_global_device_ids=true | all-gather | bytes 196608 | tf_op jit(solution)/shard_map/all_gather | solution.py:120
  21.7 4.9 %all_gather.29 = bf16[256,256]{1,0:T(8,128)(2,1)S(1)} all-gather(bf16[128,256]{1,0:T(8,128)(2,1)S(1)} %convolution_convert_fusion.2), channel_id=1, replica_groups=mesh['sp'=16,'tp'=2] {'tp'}, dimensions={0}, use_global_device_ids=true | all-gather | bytes 196608 | tf_op jit(solution)/shard_map/all_gather | solution.py:121
  26.7 7.1 %collective-permute-done = bf16[256,128]{1,0:T(8,128)(2,1)S(1)} collective-permute-done((bf16[256,128]{1,0:T(8,128)(2,1)S(1)}, bf16[256,128]{1,0:T(8,128)(2,1)S(1)}, u32[]{:S(2)}, u32[]{:S(2)}) %collective-permute-start) | collective-permute-done | bytes 65568 | tf_op jit(solution)/shard_map/ppermute | solution.py:19
  33.8 6.4 %collective-permute-done.1 = bf16[256,128]{1,0:T(8,128)(2,1)S(1)} collective-permute-done((bf16[256,128]{1,0:T(8,128)(2,1)S(1)}, bf16[256,128]{1,0:T(8,128)(2,1)S(1)}, u32[]{:S(2)}, u32[]{:S(2)}) %collective-permute-start.1) | collective-permute-done | bytes 65568 | tf_op jit(solution)/shard_map/ppermute | solution.py:19
  40.2 7.9 %collective-permute-done.2 = bf16[256,128]{1,0:T(8,128)(2,1)S(1)} collective-permute-done((bf16[256,128]{1,0:T(8,128)(2,1)S(1)}, bf16[256,128]{1,0:T(8,128)(2,1)S(1)}, u32[]{:S(2)}, u32[]{:S(2)}) %collective-permute-start.2) | collective-permute-done | bytes 65568 | tf_op jit(solution)/shard_map/ppermute | solution.py:19
  48.1 7.1 %collective-permute-done.3 = bf16[256,128]{1,0:T(8,128)(2,1)S(1)} collective-permute-done((bf16[256,128]{1,0:T(8,128)(2,1)S(1)}, bf16[256,128]{1,0:T(8,128)(2,1)S(1)}, u32[]{:S(2)}, u32[]{:S(2)}) %collective-permute-start.3) | collective-permute-done | bytes 65568 | tf_op jit(solution)/shard_map/ppermute | solution.py:19
  55.2 6.4 %collective-permute-done.4 = bf16[256,128]{1,0:T(8,128)(2,1)S(1)} collective-permute-done((bf16[256,128]{1,0:T(8,128)(2,1)S(1)}, bf16[256,128]{1,0:T(8,128)(2,1)S(1)}, u32[]{:S(2)}, u32[]{:S(2)}) %collective-permute-start.4) | collective-permute-done | bytes 65568 | tf_op jit(solution)/shard_map/ppermute | solution.py:19
  61.6 6.4 %collective-permute-done.5 = bf16[256,128]{1,0:T(8,128)(2,1)S(1)} collective-permute-done((bf16[256,128]{1,0:T(8,128)(2,1)S(1)}, bf16[256,128]{1,0:T(8,128)(2,1)S(1)}, u32[]{:S(2)}, u32[]{:S(2)}) %collective-permute-start.5) | collective-permute-done | bytes 65568 | tf_op jit(solution)/shard_map/ppermute | solution.py:19
  68.0 6.6 %collective-permute-done.6 = bf16[256,128]{1,0:T(8,128)(2,1)S(1)} collective-permute-done((bf16[256,128]{1,0:T(8,128)(2,1)S(1)}, bf16[256,128]{1,0:T(8,128)(2,1)S(1)}, u32[]{:S(2)}, u32[]{:S(2)}) %collective-permute-start.6) | collective-permute-done | bytes 65568 | tf_op jit(solution)/shard_map/ppermute | solution.py:19
  74.7 6.4 %collective-permute-done.7 = bf16[256,128]{1,0:T(8,128)(2,1)S(1)} collective-permute-done((bf16[256,128]{1,0:T(8,128)(2,1)S(1)}, bf16[256,128]{1,0:T(8,128)(2,1)S(1)}, u32[]{:S(2)}, u32[]{:S(2)}) %collective-permute-start.7) | collective-permute-done | bytes 65568 | tf_op jit(solution)/shard_map/ppermute | solution.py:19
  81.0 7.3 %collective-permute-done.8 = bf16[256,128]{1,0:T(8,128)(2,1)S(1)} collective-permute-done((bf16[256,128]{1,0:T(8,128)(2,1)S(1)}, bf16[256,128]{1,0:T(8,128)(2,1)S(1)}, u32[]{:S(2)}, u32[]{:S(2)}) %collective-permute-start.8) | collective-permute-done | bytes 65568 | tf_op jit(solution)/shard_map/ppermute | solution.py:19
  88.3 6.7 %collective-permute-done.9 = bf16[256,128]{1,0:T(8,128)(2,1)S(1)} collective-permute-done((bf16[256,128]{1,0:T(8,128)(2,1)S(1)}, bf16[256,128]{1,0:T(8,128)(2,1)S(1)}, u32[]{:S(2)}, u32[]{:S(2)}) %collective-permute-start.9) | collective-permute-done | bytes 65568 | tf_op jit(solution)/shard_map/ppermute | solution.py:19
  95.1 6.4 %collective-permute-done.10 = bf16[256,128]{1,0:T(8,128)(2,1)S(1)} collective-permute-done((bf16[256,128]{1,0:T(8,128)(2,1)S(1)}, bf16[256,128]{1,0:T(8,128)(2,1)S(1)}, u32[]{:S(2)}, u32[]{:S(2)}) %collective-permute-start.10) | collective-permute-done | bytes 65568 | tf_op jit(solution)/shard_map/ppermute | solution.py:19
  102.1 6.4 %collective-permute-done.11 = bf16[256,128]{1,0:T(8,128)(2,1)S(1)} collective-permute-done((bf16[256,128]{1,0:T(8,128)(2,1)S(1)}, bf16[256,128]{1,0:T(8,128)(2,1)S(1)}, u32[]{:S(2)}, u32[]{:S(2)}) %collective-permute-start.11) | collective-permute-done | bytes 65568 | tf_op jit(solution)/shard_map/ppermute | solution.py:19
  108.6 6.4 %collective-permute-done.12 = bf16[256,128]{1,0:T(8,128)(2,1)} collective-permute-done((bf16[256,128]{1,0:T(8,128)(2,1)S(1)}, bf16[256,128]{1,0:T(8,128)(2,1)}, u32[]{:S(2)}, u32[]{:S(2)}) %collective-permute-start.12) | collective-permute-done | bytes 65568 | tf_op jit(solution)/shard_map/ppermute | solution.py:19
  116.9 4.9 %collective-permute-done.13 = bf16[256,128]{1,0:T(8,128)(2,1)} collective-permute-done((bf16[256,128]{1,0:T(8,128)(2,1)}, bf16[256,128]{1,0:T(8,128)(2,1)}, u32[]{:S(2)}, u32[]{:S(2)}) %collective-permute-start.13) | collective-permute-done | bytes 65568 | tf_op jit(solution)/shard_map/ppermute | solution.py:19
  139.4 7.7 %while.53 = (s32[]{:T(128)}, f32[4,512,4]{1,2,0:T(4,128)S(1)}, f32[4,512,4]{1,2,0:T(4,128)S(1)}, bf16[4,512,512]{1,2,0:T(8,128)(2,1)}, bf16[256,128]{1,0:T(8,128)(2,1)S(1)}, /*index=5*/s32[]{:T(128)}) while((s32[]{:T(128)}, f32[4,512,4]{1,2,0:T(4,128)S(1)}, f32[4,512,4]{1,2,0:T(4,128)S(1)}, bf16[4,512,512]{1,2,0:T(8,128)(2,1)}, ...), condition=%wide.region_5.6_spmd, body=%wide.region_2.5_spmd.sunk | while | flops 136835072 | bytes 5890125 | solution.py:136
  147.1 18.7 %all_gather.28 = f32[16,2048,4]{1,2,0:T(4,128)S(1)} all-gather(f32[1,2048,4]{1,2,0:T(4,128)S(1)} %bitcast.179), channel_id=1, replica_groups=mesh['sp'=16,'tp'=2] {'sp'}, dimensions={0}, use_global_device_ids=true | all-gather | bytes 557056 | tf_op jit(solution)/shard_map/all_gather | solution.py:26
  165.8 20.9 %all_gather.27 = f32[16,2048,4]{1,2,0:T(4,128)S(1)} all-gather(f32[1,2048,4]{1,2,0:T(4,128)S(1)} %bitcast.178), channel_id=1, replica_groups=mesh['sp'=16,'tp'=2] {'sp'}, dimensions={0}, use_global_device_ids=true | all-gather | bytes 557056 | tf_op jit(solution)/shard_map/all_gather | solution.py:26
  187.9 24.7 %while.55 = (s32[]{:T(128)}, f32[128,4,128]{2,0,1:T(8,128)S(1)}, bf16[8,512,128]{2,1,0:T(8,128)(2,1)}, bf16[128,4,128]{2,0,1:T(8,128)(2,1)}, f32[128,4]{0,1:T(4,...) while((s32[]{:T(128)}, f32[128,4,128]{2,0,1:T(8,128)S(1)}, ...), condition=%wide.region_9.10_spmd.clone, body=%wide.region_8.9_spmd.clone.sunk | while | flops 202834432 | bytes 3285615 | solution.py:194
  214.4 17.5 %all_gather.31 = bf16[2048,4]{0,1:T(4,128)(2,1)S(1)} all-gather(bf16[128,4]{0,1:T(4,128)(2,1)S(1)} %get-tuple-element.793), channel_id=1, replica_groups=mesh['sp'=16,'tp'=2] {'sp'}, dimensions={0}, use_global_device_ids=true | all-gather | bytes 17408 | tf_op jit(solution)/shard_map/all_gather | solution.py:152
  234.7 40.6 %while.56 = (s32[]{:T(128)}, f32[256,128]{1,0:T(8,128)S(1)}, f32[256,128]{1,0:T(8,128)S(1)}, bf16[4,512,512]{1,2,0:T(8,128)(2,1)}, bf16[256,128]{1,0:T(8,128)(2,...) while((s32[]{:T(128)}, f32[256,128]{1,0:T(8,128)S(1)}, ...), condition=%wide.region_13.14_spmd.clone, body=%wide.region_12.13_spmd.clone.sunk | while | flops 541231104 | bytes 14340260 | solution.py:165
  275.6 7.1 %all_to_all.5 = bf16[2,128,256]{2,1,0:T(8,128)(2,1)S(1)} all-to-all(bf16[2,128,256]{2,1,0:T(8,128)(2,1)S(1)} %convert_element_type.103), channel_id=1, replica_groups=mesh['sp'=16,'tp'=2] {'tp'}, dimensions={0} | all-to-all | bytes 262144 | tf_op jit(solution)/shard_map/all_to_all | solution.py:206
  290.5 27.2 %reduce-scatter.2.cloned.1.call-done = f32[128,512]{1,0:T(8,128)} async-done(((f32[2048,512]{1,0:T(8,128)}), f32[128,512]{1,0:T(8,128)}) %reduce-scatter.2.cloned.1.call-update) | async-done | bytes 262160 | tf_op jit(solution)/shard_map/reduce_scatter | solution.py:196
  (247 shorter events, 115.4 us)
Async XLA Ops:
  7.2 128.0 %all-gather.6.cloned.1.call-start = ((), (), s32[]{:S(2)}) async-start(), calls=%async_computation.3 | async-start | bytes 2228224 | tf_op jit(solution)/shard_map/all_gather | solution.py:133
  11.1 176.7 %all-gather.4.cloned.1.call-start = ((), (), s32[]{:S(2)}) async-start(), calls=%async_computation.2 | async-start | bytes 1114112 | tf_op jit(solution)/shard_map/all_gather | solution.py:175
  11.9 103.1 %copy-start.9 = (bf16[128,512]{1,0:T(8,128)(2,1)S(1)}, bf16[128,512]{1,0:T(8,128)(2,1)}, u32[]{:S(2)}) copy-start(bf16[128,512]{1,0:T(8,128)(2,1)} %convolution_convert_fusion.1) | copy-start | bytes 393220
  11.9 103.7 %copy-start.8 = (bf16[128,512]{1,0:T(8,128)(2,1)S(1)}, bf16[128,512]{1,0:T(8,128)(2,1)}, u32[]{:S(2)}) copy-start(bf16[128,512]{1,0:T(8,128)(2,1)} %param.25) | copy-start | bytes 393220
  20.1 214.6 %all-gather.8.cloned.1.call-start = ((), (), s32[]{:S(2)}) async-start(), calls=%async_computation.5 | async-start | bytes 2228224 | tf_op jit(solution)/shard_map/all_gather | solution.py:151
  26.7 81.8 %copy-start.15 = (bf16[256,128]{1,0:T(8,128)(2,1)}, bf16[256,128]{1,0:T(8,128)(2,1)S(1)}, u32[]{:S(2)}) copy-start(bf16[256,128]{1,0:T(8,128)(2,1)S(1)} %constant_dynamic-slice_fusion.4) | copy-start | bytes 196612
  26.7 7.1 %collective-permute-start = (bf16[256,128]{1,0:T(8,128)(2,1)S(1)}, bf16[256,128]{1,0:T(8,128)(2,1)S(1)}, u32[]{:S(2)}, u32[]{:S(2)}) collective-permute-start(bf16[256,128]{1,0:T(8,128)(2,1)S(1)} %constant_dynamic-slice_fusion.4), channel_id=1, source_target_pairs={{0,2},{2,4},{4,6},{6,8},{8,10},{10,12},{12,14},{14,16},{16,18},{18... | collective-permute-start | bytes 196616 | tf_op jit(solution)/shard_map/ppermute | solution.py:19
  33.8 6.4 %collective-permute-start.1 = (bf16[256,128]{1,0:T(8,128)(2,1)S(1)}, bf16[256,128]{1,0:T(8,128)(2,1)S(1)}, u32[]{:S(2)}, u32[]{:S(2)}) collective-permute-start(bf16[256,128]{1,0:T(8,128)(2,1)S(1)} %collective-permute-done), channel_id=1, source_target_pairs={{0,2},{2,4},{4,6},{6,8},{8,10},{10,12},{12,14},{14,16},{16,18},{18... | collective-permute-start | bytes 196616 | tf_op jit(solution)/shard_map/ppermute | solution.py:19
  40.2 7.9 %collective-permute-start.2 = (bf16[256,128]{1,0:T(8,128)(2,1)S(1)}, bf16[256,128]{1,0:T(8,128)(2,1)S(1)}, u32[]{:S(2)}, u32[]{:S(2)}) collective-permute-start(bf16[256,128]{1,0:T(8,128)(2,1)S(1)} %collective-permute-done.1), channel_id=1, source_target_pairs={{0,2},{2,4},{4,6},{6,8},{8,10},{10,12},{12,14},{14,16},{16,18},{18... | collective-permute-start | bytes 196616 | tf_op jit(solution)/shard_map/ppermute | solution.py:19
  48.1 7.1 %collective-permute-start.3 = (bf16[256,128]{1,0:T(8,128)(2,1)S(1)}, bf16[256,128]{1,0:T(8,128)(2,1)S(1)}, u32[]{:S(2)}, u32[]{:S(2)}) collective-permute-start(bf16[256,128]{1,0:T(8,128)(2,1)S(1)} %collective-permute-done.2), channel_id=1, source_target_pairs={{0,2},{2,4},{4,6},{6,8},{8,10},{10,12},{12,14},{14,16},{16,18},{18... | collective-permute-start | bytes 196616 | tf_op jit(solution)/shard_map/ppermute | solution.py:19
  55.2 6.4 %collective-permute-start.4 = (bf16[256,128]{1,0:T(8,128)(2,1)S(1)}, bf16[256,128]{1,0:T(8,128)(2,1)S(1)}, u32[]{:S(2)}, u32[]{:S(2)}) collective-permute-start(bf16[256,128]{1,0:T(8,128)(2,1)S(1)} %collective-permute-done.3), channel_id=1, source_target_pairs={{0,2},{2,4},{4,6},{6,8},{8,10},{10,12},{12,14},{14,16},{16,18},{18... | collective-permute-start | bytes 196616 | tf_op jit(solution)/shard_map/ppermute | solution.py:19
  61.6 6.4 %collective-permute-start.5 = (bf16[256,128]{1,0:T(8,128)(2,1)S(1)}, bf16[256,128]{1,0:T(8,128)(2,1)S(1)}, u32[]{:S(2)}, u32[]{:S(2)}) collective-permute-start(bf16[256,128]{1,0:T(8,128)(2,1)S(1)} %collective-permute-done.4), channel_id=1, source_target_pairs={{0,2},{2,4},{4,6},{6,8},{8,10},{10,12},{12,14},{14,16},{16,18},{18... | collective-permute-start | bytes 196616 | tf_op jit(solution)/shard_map/ppermute | solution.py:19
  68.0 6.6 %collective-permute-start.6 = (bf16[256,128]{1,0:T(8,128)(2,1)S(1)}, bf16[256,128]{1,0:T(8,128)(2,1)S(1)}, u32[]{:S(2)}, u32[]{:S(2)}) collective-permute-start(bf16[256,128]{1,0:T(8,128)(2,1)S(1)} %collective-permute-done.5), channel_id=1, source_target_pairs={{0,2},{2,4},{4,6},{6,8},{8,10},{10,12},{12,14},{14,16},{16,18},{18... | collective-permute-start | bytes 196616 | tf_op jit(solution)/shard_map/ppermute | solution.py:19
  74.6 6.4 %collective-permute-start.7 = (bf16[256,128]{1,0:T(8,128)(2,1)S(1)}, bf16[256,128]{1,0:T(8,128)(2,1)S(1)}, u32[]{:S(2)}, u32[]{:S(2)}) collective-permute-start(bf16[256,128]{1,0:T(8,128)(2,1)S(1)} %collective-permute-done.6), channel_id=1, source_target_pairs={{0,2},{2,4},{4,6},{6,8},{8,10},{10,12},{12,14},{14,16},{16,18},{18... | collective-permute-start | bytes 196616 | tf_op jit(solution)/shard_map/ppermute | solution.py:19
  81.0 7.3 %collective-permute-start.8 = (bf16[256,128]{1,0:T(8,128)(2,1)S(1)}, bf16[256,128]{1,0:T(8,128)(2,1)S(1)}, u32[]{:S(2)}, u32[]{:S(2)}) collective-permute-start(bf16[256,128]{1,0:T(8,128)(2,1)S(1)} %collective-permute-done.7), channel_id=1, source_target_pairs={{0,2},{2,4},{4,6},{6,8},{8,10},{10,12},{12,14},{14,16},{16,18},{18... | collective-permute-start | bytes 196616 | tf_op jit(solution)/shard_map/ppermute | solution.py:19
  88.3 6.7 %collective-permute-start.9 = (bf16[256,128]{1,0:T(8,128)(2,1)S(1)}, bf16[256,128]{1,0:T(8,128)(2,1)S(1)}, u32[]{:S(2)}, u32[]{:S(2)}) collective-permute-start(bf16[256,128]{1,0:T(8,128)(2,1)S(1)} %collective-permute-done.8), channel_id=1, source_target_pairs={{0,2},{2,4},{4,6},{6,8},{8,10},{10,12},{12,14},{14,16},{16,18},{18... | collective-permute-start | bytes 196616 | tf_op jit(solution)/shard_map/ppermute | solution.py:19
  95.1 6.4 %collective-permute-start.10 = (bf16[256,128]{1,0:T(8,128)(2,1)S(1)}, bf16[256,128]{1,0:T(8,128)(2,1)S(1)}, u32[]{:S(2)}, u32[]{:S(2)}) collective-permute-start(bf16[256,128]{1,0:T(8,128)(2,1)S(1)} %collective-permute-done.9), channel_id=1, source_target_pairs={{0,2},{2,4},{4,6},{6,8},{8,10},{10,12},{12,14},{14,16},{16,18},{18... | collective-permute-start | bytes 196616 | tf_op jit(solution)/shard_map/ppermute | solution.py:19
  102.1 6.4 %collective-permute-start.11 = (bf16[256,128]{1,0:T(8,128)(2,1)S(1)}, bf16[256,128]{1,0:T(8,128)(2,1)S(1)}, u32[]{:S(2)}, u32[]{:S(2)}) collective-permute-start(bf16[256,128]{1,0:T(8,128)(2,1)S(1)} %collective-permute-done.10), channel_id=1, source_target_pairs={{0,2},{2,4},{4,6},{6,8},{8,10},{10,12},{12,14},{14,16},{16,18},{18... | collective-permute-start | bytes 196616 | tf_op jit(solution)/shard_map/ppermute | solution.py:19
  108.5 6.5 %collective-permute-start.12 = (bf16[256,128]{1,0:T(8,128)(2,1)S(1)}, bf16[256,128]{1,0:T(8,128)(2,1)}, u32[]{:S(2)}, u32[]{:S(2)}) collective-permute-start(bf16[256,128]{1,0:T(8,128)(2,1)S(1)} %collective-permute-done.11), channel_id=1, source_target_pairs={{0,2},{2,4},{4,6},{6,8},{8,10},{10,12},{12,14},{14,16},{16,18},{18... | collective-permute-start | bytes 196616 | tf_op jit(solution)/shard_map/ppermute | solution.py:19
  108.5 178.5 %all-reduce.2.cloned.1.call-start = ((), (), s32[]{:S(2)}) async-start(), calls=%async_computation.4 | async-start | bytes 1048576 | tf_op jit(solution)/shard_map/psum | solution.py:203
  115.0 6.8 %collective-permute-start.13 = (bf16[256,128]{1,0:T(8,128)(2,1)}, bf16[256,128]{1,0:T(8,128)(2,1)}, u32[]{:S(2)}, u32[]{:S(2)}) collective-permute-start(bf16[256,128]{1,0:T(8,128)(2,1)} %collective-permute-done.12), channel_id=1, source_target_pairs={{0,2},{2,4},{4,6},{6,8},{8,10},{10,12},{12,14},{14,16},{16,18},{18... | collective-permute-start | bytes 196616 | tf_op jit(solution)/shard_map/ppermute | solution.py:19
  121.8 6.7 %collective-permute-start.14 = (bf16[256,128]{1,0:T(8,128)(2,1)}, bf16[256,128]{1,0:T(8,128)(2,1)}, u32[]{:S(2)}, u32[]{:S(2)}) collective-permute-start(bf16[256,128]{1,0:T(8,128)(2,1)} %collective-permute-done.13), channel_id=1, source_target_pairs={{0,2},{2,4},{4,6},{6,8},{8,10},{10,12},{12,14},{14,16},{16,18},{18... | collective-permute-start | bytes 196616 | tf_op jit(solution)/shard_map/ppermute | solution.py:19
  212.5 19.3 %copy-start.3 = (bf16[128,2048]{1,0:T(8,128)(2,1)S(1)}, bf16[128,2048]{1,0:T(8,128)(2,1)}, u32[]{:S(2)}) copy-start(bf16[128,2048]{1,0:T(8,128)(2,1)} %param.17) | copy-start | bytes 1572868
  214.3 103.4 %reduce-scatter.2.cloned.1.call-start = ((), (), s32[]{:S(2)}) async-start(), calls=%async_computation.6 | async-start | bytes 4456448 | tf_op jit(solution)/shard_map/reduce_scatter | solution.py:196
  (22 other events, 114.2 us)
Sparse Core Ops, SparseCore 0:
  11.3 44.9 all-gather.5
  58.4 37.4 all-gather.3
  108.6 43.0 all-gather.7
  214.4 26.1 all-reduce.1
  244.9 72.7 reduce-scatter.1
